TPU v7x, 32 devices: a whole 2x2x4 slice. The times are simulated.
32 devices in a mesh: grp: 2 (over y), sp: 4 (over z), tp: 4 (over x, core).
Axes of the slice: x: 2, y: 2, z: 4, core: 2. Of those that a mesh axis runs over, the one named last changes fastest.
Arguments:
- query_nope: bfloat16 [2560, 1024], P(('grp', 'sp'), 'tp'), parts along dimension 0, may hold values from -12 to 12
- query_rope: bfloat16 [2560, 512], P(('grp', 'sp'), 'tp'), parts along dimension 0, may hold values from -48 to 48
- token_latent: bfloat16 [2560, 256], P(('grp', 'sp')), parts along dimension 0, may hold values from -6 to 6
- key_rope: bfloat16 [2560, 32], P(('grp', 'sp')), parts along dimension 0, may hold values from -48 to 48
- latent_norm_gain: float32 [256], replicated, may hold values from 0.1 to 1.9
- key_expand_weight: bfloat16 [256, 1024], replicated, may hold values from -0.375 to 0.375
- value_expand_weight: bfloat16 [256, 1024], replicated, may hold values from -0.375 to 0.375
- residual: bfloat16 [2560, 2048], P(('grp', 'sp')), parts along dimension 0, may hold values from -3 to 3
- out_weight: bfloat16 [1024, 2048], P('tp'), may hold values from -0.375 to 0.375
- ffn_gain: float32 [2048], replicated, may hold values from 0.1 to 1.9
- gate_weight: bfloat16 [2048, 5632], P('sp', 'tp'), may hold values from -0.125 to 0.125
- up_weight: bfloat16 [2048, 5632], P('sp', 'tp'), may hold values from -0.125 to 0.125
- down_weight: bfloat16 [5632, 2048], P('tp', 'sp'), may hold values from -0.078125 to 0.078125
Outputs:
- layer_output: bfloat16 [2560, 2048], P(('grp', 'sp', 'tp')), parts along dimension 0
There are 2 independent parts, one for each index of `grp`. A program takes and returns all parts, laid end to end along the dimension named above; an argument that names none is the same for every part. Nothing has to cross between parts.
All inputs are finite; a program needn't handle non-finite values.
Results may differ from a plain program's by a relative error of at most 0.015.
Values may be sent and summed in bfloat16 or wider, within the bound.
A program may use at most 128 MiB of HBM per device.

v0:
```python
import jax
import jax.numpy as jnp
from jax import lax
from jax.sharding import PartitionSpec as P

UNROTATED_SIZE = 64
ROPE = 32
VALUE_SIZE = 64
GRID_W = 64


def norm_rows(values, gain):
    wide = values.astype(jnp.float32)
    return wide * lax.rsqrt(jnp.mean(wide * wide, axis=-1, keepdims=True) + 1e-06) * gain


def turn_heads(vectors, positions):
    tokens, heads, width = vectors.shape
    freqs = width // 4
    grid_pos = jnp.stack([positions // GRID_W, positions % GRID_W], axis=-1).astype(jnp.float32)
    inverse = jnp.power(10000.0, -jnp.arange(freqs, dtype=jnp.float32) / freqs)
    angles = grid_pos[:, :, None] * inverse
    cosine = jnp.cos(angles)[:, None]
    sine = jnp.sin(angles)[:, None]
    viewed = vectors.reshape(tokens, heads, 2, 2, freqs)
    first = viewed[..., 0, :]
    second = viewed[..., 1, :]
    turned = jnp.stack([first * cosine - second * sine, first * sine + second * cosine], axis=-2)
    return turned.reshape(tokens, heads, width)


def local(
    query_nope,
    query_rope,
    token_latent,
    key_rope,
    latent_norm_gain,
    key_expand_weight,
    value_expand_weight,
    residual,
    out_weight,
    ffn_gain,
    gate_weight,
    up_weight,
    down_weight,
):
    tok_rows = query_nope.shape[0]
    heads_here = query_nope.shape[1] // UNROTATED_SIZE
    own_rows = tok_rows // lax.axis_size("tp")
    tp_index = lax.axis_index("tp")
    positions = lax.axis_index("sp") * tok_rows + jnp.arange(tok_rows, dtype=jnp.int32)
    query_flat = query_nope.reshape(tok_rows, heads_here, UNROTATED_SIZE)
    query_turned = turn_heads(
        query_rope.astype(jnp.float32).reshape(tok_rows, heads_here, ROPE), positions
    ).astype(jnp.bfloat16)
    latent = norm_rows(token_latent, latent_norm_gain).astype(jnp.bfloat16)
    key_turned = turn_heads(key_rope.astype(jnp.float32)[:, None, :], positions)[:, 0].astype(
        jnp.bfloat16
    )
    key_cols = lax.dynamic_slice_in_dim(
        key_expand_weight, tp_index * heads_here * UNROTATED_SIZE, heads_here * UNROTATED_SIZE, 1
    )
    value_cols = lax.dynamic_slice_in_dim(
        value_expand_weight, tp_index * heads_here * VALUE_SIZE, heads_here * VALUE_SIZE, 1
    )
    score_scale = (UNROTATED_SIZE + ROPE) ** (-0.5)

    def absorb(carried, block_in):
        latent_block, rope_block = block_in
        block_rows = latent_block.shape[0]
        key_rows = jnp.dot(latent_block, key_cols, preferred_element_type=jnp.float32).astype(
            jnp.bfloat16
        )
        key_rows = key_rows.reshape(block_rows, heads_here, UNROTATED_SIZE)
        value_rows = jnp.dot(latent_block, value_cols, preferred_element_type=jnp.float32).astype(
            jnp.bfloat16
        )
        value_rows = value_rows.reshape(block_rows, heads_here, VALUE_SIZE)
        scores = (
            jnp.einsum("qhd,khd->hqk", query_flat, key_rows, preferred_element_type=jnp.float32)
            + jnp.einsum(
                "qhd,kd->hqk", query_turned, rope_block, preferred_element_type=jnp.float32
            )
        ) * score_scale
        highest, totals, accumulated = carried
        new_highest = jnp.maximum(highest, jnp.max(scores, axis=-1))
        shrink = jnp.exp(highest - new_highest)
        weights = jnp.exp(scores - new_highest[:, :, None])
        totals = totals * shrink + jnp.sum(weights, axis=-1)
        accumulated = accumulated * shrink.T[:, :, None] + jnp.einsum(
            "hqk,khd->qhd",
            weights.astype(jnp.bfloat16),
            value_rows,
            preferred_element_type=jnp.float32,
        )
        return ((new_highest, totals, accumulated), None)

    initial = (
        jnp.full((heads_here, tok_rows), -jnp.inf, jnp.float32),
        jnp.zeros((heads_here, tok_rows), jnp.float32),
        jnp.zeros((tok_rows, heads_here, VALUE_SIZE), jnp.float32),
    )
    carried = initial
    latent_piece = lax.all_gather(latent, "sp", axis=0, tiled=True)
    rope_piece = lax.all_gather(key_turned, "sp", axis=0, tiled=True)
    shard_count = latent_piece.shape[0] // tok_rows
    grouped = max(
        (
            factor
            for factor in range(1, shard_count + 1)
            if shard_count % factor == 0 and factor * tok_rows <= max(1024, tok_rows)
        )
    )
    block_rows = grouped * tok_rows
    blocks = (
        latent_piece.reshape(-1, block_rows, latent_piece.shape[1]),
        rope_piece.reshape(-1, block_rows, rope_piece.shape[1]),
    )
    carried, _ = lax.scan(absorb, carried, blocks)
    highest, totals, accumulated = carried
    attended = (
        (accumulated / totals.T[:, :, None])
        .reshape(tok_rows, heads_here * VALUE_SIZE)
        .astype(jnp.bfloat16)
    )
    projected = jnp.dot(attended, out_weight, preferred_element_type=jnp.float32).astype(
        jnp.bfloat16
    )
    summed = lax.psum(projected, "tp").astype(jnp.float32)
    mixed_all = residual.astype(jnp.float32) + summed
    normed_all = norm_rows(mixed_all, ffn_gain).astype(jnp.bfloat16)
    mixed_own = lax.dynamic_slice_in_dim(mixed_all, tp_index * own_rows, own_rows, 0)
    gate_piece = lax.all_gather(gate_weight, "sp", axis=0, tiled=True)
    up_piece = lax.all_gather(up_weight, "sp", axis=0, tiled=True)
    gate = jnp.dot(normed_all, gate_piece, preferred_element_type=jnp.float32)
    up_part = jnp.dot(normed_all, up_piece, preferred_element_type=jnp.float32)
    hidden = (jax.nn.silu(gate) * up_part).astype(jnp.bfloat16)
    terms = jnp.dot(
        hidden,
        lax.all_gather(down_weight, "sp", axis=1, tiled=True),
        preferred_element_type=jnp.float32,
    )
    ffn_own = lax.psum_scatter(
        terms.astype(jnp.bfloat16), "tp", scatter_dimension=0, tiled=True
    ).astype(jnp.float32)
    return (mixed_own + ffn_own).astype(jnp.bfloat16)


def solution(mesh):
    return jax.shard_map(
        local,
        mesh=mesh,
        in_specs=(
            P(("grp", "sp"), "tp"),
            P(("grp", "sp"), "tp"),
            P(("grp", "sp"), None),
            P(("grp", "sp"), None),
            P(),
            P(),
            P(),
            P(("grp", "sp"), None),
            P("tp", None),
            P(),
            P("sp", "tp"),
            P("sp", "tp"),
            P("tp", "sp"),
        ),
        out_specs=P(("grp", "sp", "tp"), None),
        check_vma=False,
    )
```

profile of v0, /device:TPU:0, one launch (start us, length us, event | category | flops | bytes accessed | tf_op | source)
XLA Modules:
  0.0 428.1 jit_solution(11533256106749414533)
XLA Ops:
  7.4 1.1 copy.26
  8.6 0.7 convert.18
  9.7 15.1 %all-gather = bf16[4,320,32]{1,2,0:T(8,128)(2,1)S(1)} all-gather(bf16[1,320,32]{1,2,0:T(8,128)(2,1)S(1)} %bitcast.82), channel_id=1, replica_groups=mesh['grp'=2,'sp'=4,'tp'=4] {'sp'}, dimensions={0}, use_global_device_ids=true | all-gather | bytes 102400 | tf_op jit(solution)/shard_map/all_gather | solution.py:105
  25.0 1.1 fusion.24
  26.1 1.0 fusion.26
  27.1 16.8 %all_gather.15 = bf16[1280,256]{1,0:T(8,128)(2,1)S(1)} all-gather(bf16[320,256]{1,0:T(8,128)(2,1)S(1)} %fusion.26), channel_id=1, replica_groups=mesh['grp'=2,'sp'=4,'tp'=4] {'sp'}, dimensions={0}, use_global_device_ids=true | all-gather | bytes 819200 | tf_op jit(solution)/shard_map/all_gather | solution.py:104
  44.2 1.0 constant_dynamic-slice_fusion
  45.2 15.2 %while.15 = (s32[]{:T(128)}, f32[4,320]{1,0:T(4,128)S(1)}, f32[4,320]{1,0:T(4,128)S(1)}, f32[320,4,64]{0,2,1:T(8,128)S(1)}, bf16[2,640,256]{2,1,0:T(8,128)(2,1)S...) while((s32[]{:T(128)}, f32[4,320]{1,0:T(4,128)S(1)}, ...), condition=%wide.region_4.5_spmd.clone, body=%wide.region_1.4_spmd.clone.sunk | while | flops 436231680 | bytes 32759976 | solution.py:119
  46.1 2.4 fusion.75
  48.8 2.9 fusion.79
  51.8 1.0 fusion.77
  53.7 2.4 fusion.75
  56.4 2.9 fusion.79
  59.3 1.0 fusion.77
  60.4 1.6 convolution_convert_fusion.3
  63.9 37.3 %all-reduce.2.cloned.1.call-done = bf16[320,2048]{1,0:T(8,128)(2,1)} async-done(((bf16[320,2048]{1,0:T(8,128)(2,1)}), bf16[320,2048]{1,0:T(8,128)(2,1)}) %all-reduce.2.cloned.1.call-update) | async-done | bytes 1310736 | tf_op jit(solution)/shard_map/psum | solution.py:129
  101.1 3.2 convert_add_fusion
  104.4 66.1 %all-gather.5.cloned.1.call-done = bf16[2048,1408]{1,0:T(8,128)(2,1)} async-done(((bf16[512,1408]{1,0:T(8,128)(2,1)}), bf16[2048,1408]{1,0:T(8,128)(2,1)}) %all-gather.5.cloned.1.call-update) | async-done | bytes 5767184 | tf_op jit(solution)/shard_map/all_gather | solution.py:133
  170.5 6.5 %fusion.36 = f32[320,1408]{1,0:T(8,128)} fusion(bf16[2048,1408]{1,0:T(8,128)(2,1)} %all-gather.5.cloned.1.call-done, f32[2048]{0:T(1024)S(1)} %copy-done.4, f32[320]{0:T(512)S(1)} %add_rsqrt_fusion, bf16[320,2048]{1,0:T(8,128)(2,1)} %all-reduce.2.cloned.1.call-done, bf16[320,2048]{1,0:T(8,128)(2,1)S(1)} %copy-done.2), kind=kOutput, calls=%fused_computation.69 | convolution fusion | flops 1849425920 | bytes 10200320 | tf_op jit(solution)/shard_map/dot_general | solution.py:135
  177.0 99.7 %all-gather.7.cloned.1.call-done = bf16[2048,1408]{1,0:T(8,128)(2,1)} async-done(((bf16[512,1408]{1,0:T(8,128)(2,1)}), bf16[2048,1408]{1,0:T(8,128)(2,1)}) %all-gather.7.cloned.1.call-update) | async-done | bytes 5767184 | tf_op jit(solution)/shard_map/all_gather | solution.py:134
  276.8 106.3 %all-gather.9.cloned.1.call-done = bf16[1408,2048]{1,0:T(8,128)(2,1)} async-done(((bf16[1408,512]{1,0:T(8,128)(2,1)}), bf16[1408,2048]{1,0:T(8,128)(2,1)}) %all-gather.9.cloned.1.call-update) | async-done | bytes 5767184 | tf_op jit(solution)/shard_map/all_gather | solution.py:140
  383.0 10.7 %convolution_convert_fusion.2 = bf16[320,2048]{1,0:T(8,128)(2,1)} fusion(bf16[1408,2048]{1,0:T(8,128)(2,1)} %all-gather.9.cloned.1.call-done, bf16[2048,1408]{1,0:T(8,128)(2,1)} %all-gather.7.cloned.1.call-done, f32[320,1408]{1,0:T(8,128)} %fusion.36, f32[2048]{0:T(1024)S(1)} %copy-done.4, f32[320]{0:T(512)S(1)} %add_rsqrt_fusion, ...), kind=kOutput, calls=%fused_computation.27 | convolution fusion | flops 3698278400 | bytes 17278208 | tf_op jit(solution)/shard_map/dot_general | solution.py:138
  393.7 24.8 %reduce-scatter.2.cloned.1.call-done = bf16[80,2048]{1,0:T(8,128)(2,1)} async-done(((bf16[320,2048]{1,0:T(8,128)(2,1)}), bf16[80,2048]{1,0:T(8,128)(2,1)}) %reduce-scatter.2.cloned.1.call-update) | async-done | bytes 327696 | tf_op jit(solution)/shard_map/reduce_scatter | solution.py:143
  418.6 2.0 add_convert_fusion
  (53 shorter events, 5.3 us)
Async XLA Ops:
  7.4 53.0 %copy-start = (bf16[256,2048]{1,0:T(8,128)(2,1)S(1)}, bf16[256,2048]{1,0:T(8,128)(2,1)}, u32[]{:S(2)}) copy-start(bf16[256,2048]{1,0:T(8,128)(2,1)} %param.23) | copy-start | bytes 3145732
  7.4 36.6 %copy-start.3 = (bf16[320,256]{1,0:T(8,128)(2,1)S(1)}, bf16[320,256]{1,0:T(8,128)(2,1)}, u32[]{:S(2)}) copy-start(bf16[320,256]{1,0:T(8,128)(2,1)} %param.15) | copy-start | bytes 491524
  7.4 93.8 %all-reduce.2.cloned.1.call-start = ((), (), s32[]{:S(2)}) async-start(), calls=%async_computation.1 | async-start | bytes 2621440 | tf_op jit(solution)/shard_map/psum | solution.py:129
  48.5 3.2 copy-start.1
  56.1 3.2 copy-start.1
  62.0 39.1 %copy-start.2 = (bf16[320,2048]{1,0:T(8,128)(2,1)S(1)}, bf16[320,2048]{1,0:T(8,128)(2,1)}, u32[]{:S(2)}) copy-start(bf16[320,2048]{1,0:T(8,128)(2,1)} %param.22) | copy-start | bytes 3932164
  62.1 108.4 %all-gather.5.cloned.1.call-start = ((), (), s32[]{:S(2)}) async-start(), calls=%async_computation.2 | async-start | bytes 7208960 | tf_op jit(solution)/shard_map/all_gather | solution.py:133
  62.6 214.1 %all-gather.7.cloned.1.call-start = ((), (), s32[]{:S(2)}) async-start(), calls=%async_computation.3 | async-start | bytes 7208960 | tf_op jit(solution)/shard_map/all_gather | solution.py:134
  63.2 319.8 %all-gather.9.cloned.1.call-start = ((), (), s32[]{:S(2)}) async-start(), calls=%async_computation.4 | async-start | bytes 7208960 | tf_op jit(solution)/shard_map/all_gather | solution.py:140
  63.8 106.7 %copy-start.4 = (f32[2048]{0:T(1024)S(1)}, f32[2048]{0:T(1024)}, u32[]{:S(2)}) copy-start(f32[2048]{0:T(1024)} %param.24) | copy-start | bytes 24580
  63.8 354.8 %reduce-scatter.2.cloned.1.call-start = ((), (), s32[]{:S(2)}) async-start(), calls=%async_computation.5 | async-start | bytes 1638400 | tf_op jit(solution)/shard_map/reduce_scatter | solution.py:143
Sparse Core Ops, SparseCore 0:
  62.2 38.9 all-reduce.1
  393.8 24.6 reduce-scatter.1
Sparse Core Ops, SparseCore 1:
  64.1 106.3 all-gather.4
  171.9 104.8 all-gather.6
  278.2 104.8 all-gather.8
where the time goes:
time: 428 us
  waiting for transfers between devices  336 us (79%)
  blocking collectives  31.9 us (7%)
  matrix products  31.9 us (7%)
  between operations  15.2 us (4%)
  other arithmetic  10.5 us (2%)
    all_gather x1, waiting for transfers between devices, local(): lax.all_gather(down_weight, 'sp', axis=1, tiled=True)  106 us
    all_gather x1, waiting for transfers between devices, local(): up_piece = lax.all_gather(up_weight, 'sp', axis=0, tiled=True)  99.7 us
    all_gather x1, waiting for transfers between devices, local(): gate_piece = lax.all_gather(gate_weight, 'sp', axis=0, tiled=True)  66.1 us
    psum x1, waiting for transfers between devices, local(): summed = lax.psum(projected, 'tp').astype(jnp.float32)  37.3 us
    reduce_scatter x1, waiting for transfers between devices, local(): lax.psum_scatter(terms.astype(jnp.bfloat16), 'tp', scatter_dimension=0, t...  24.8 us
    all_gather x1, blocking collectives, local(): latent_piece = lax.all_gather(latent, 'sp', axis=0, tiled=True)  16.8 us
    all_gather x1, blocking collectives, local(): rope_piece = lax.all_gather(key_turned, 'sp', axis=0, tiled=True)  15.1 us
    dot_general x1, matrix products, local(): jnp.dot(hidden, lax.all_gather(down_weight, 'sp', axis=1, tiled=True), pr...  10.7 us
  transfers between devices with their start and end apart: 5, of which 5 were waited for; matrix products, arithmetic and copies ran while one was open for 2% of the time, Pallas kernels for 0%

commit v1 on v0

--- a/solution.py
+++ b/solution.py
@@ -1,8 +1,13 @@
+import functools
+
 import jax
 import jax.numpy as jnp
 from jax import lax
+from jax.experimental import pallas as pl
+from jax.experimental.pallas import tpu as pltpu
 from jax.sharding import PartitionSpec as P
 
+MESH = pl.DeviceIdType.MESH
 UNROTATED_SIZE = 64
 ROPE = 32
 VALUE_SIZE = 64
@@ -27,6 +32,270 @@
     second = viewed[..., 1, :]
     turned = jnp.stack([first * cosine - second * sine, first * sine + second * cosine], axis=-2)
     return turned.reshape(tokens, heads, width)
+
+
+def spread_hidden(token_count, hidden_columns):
+    fits = lax.axis_size("tp") == 4 and lax.axis_size("grp") == 2
+    return fits and 2 * token_count < 3 * hidden_columns
+
+
+def column_tiles(hidden_columns):
+    tiles = hidden_columns // 128
+    return tiles, -(-tiles // lax.axis_size("sp"))
+
+
+def window_start(at, hidden_columns):
+    tiles, per = column_tiles(hidden_columns)
+    return lax.div(at * (tiles - per), lax.axis_size("sp") - 1)
+
+
+def signal_all(peers):
+    barrier = pltpu.get_barrier_semaphore()
+    for peer in peers:
+        pl.semaphore_signal(barrier, inc=1, device_id=peer, device_id_type=MESH)
+    pl.semaphore_wait(barrier, len(peers))
+
+
+def remote(src, dst, send_sem, recv_sem, peer):
+    return pltpu.make_async_remote_copy(
+        src_ref=src,
+        dst_ref=dst,
+        send_sem=send_sem,
+        recv_sem=recv_sem,
+        device_id=peer,
+        device_id_type=MESH,
+    )
+
+
+def weights_kernel(
+    size, hidden_columns, gate, up, down, gate_out, up_out, down_out,
+    own_sem, z_send, z_recv, y_send, y_recv,
+):
+    here = lax.axis_index("sp")
+    part = lax.axis_index("grp")
+    depth = gate.shape[0]
+    width = gate_out.shape[1]
+    outer = down.shape[1]
+
+    def start_of(at):
+        return pl.multiple_of(window_start(at, hidden_columns) * 128, 128)
+
+    def piece(out, kind, origin, half):
+        if kind < 2:
+            rows = depth // 2
+            return out.at[pl.ds(pl.multiple_of(origin * depth + half * rows, rows), rows), :]
+        rows = width // 2
+        return out.at[
+            pl.ds(pl.multiple_of(half * rows, rows), rows),
+            pl.ds(pl.multiple_of(origin * outer, outer), outer),
+        ]
+
+    def source(ref, kind, target, half):
+        if kind < 2:
+            rows = depth // 2
+            return ref.at[pl.ds(pl.multiple_of(half * rows, rows), rows), pl.ds(start_of(target), width)]
+        rows = width // 2
+        return ref.at[pl.ds(pl.multiple_of(start_of(target) + half * rows, 64), rows), :]
+
+    peers = [{"sp": lax.rem(here + shift, size)} for shift in range(1, size)]
+    signal_all(peers + [{"grp": 1 - part}])
+    refs = ((gate, gate_out), (up, up_out), (down, down_out))
+    across = []
+    for kind, (ref, out) in enumerate(refs):
+        for shift in range(1, size):
+            target = lax.rem(here + shift, size)
+            copy = remote(
+                source(ref, kind, target, part),
+                piece(out, kind, here, part),
+                z_send.at[kind, shift - 1],
+                z_recv.at[kind, shift - 1],
+                {"sp": target},
+            )
+            copy.start()
+            across.append(copy)
+    locals_ = []
+    for kind, (ref, out) in enumerate(refs):
+        for half in range(2):
+            copy = pltpu.make_async_copy(
+                source(ref, kind, here, half), piece(out, kind, here, half), own_sem.at[kind, half]
+            )
+            copy.start()
+            locals_.append(copy)
+    swaps = []
+    for kind, (ref, out) in enumerate(refs):
+        for shift in range(1, size):
+            origin = lax.rem(here - shift + size, size)
+            across[kind * (size - 1) + shift - 1].wait_recv()
+            held = piece(out, kind, origin, part)
+            copy = remote(
+                held, held, y_send.at[kind, shift - 1], y_recv.at[kind, shift - 1], {"grp": 1 - part}
+            )
+            copy.start()
+            swaps.append(copy)
+    for copy in across:
+        copy.wait_send()
+    for copy in locals_:
+        copy.wait()
+    for copy in swaps:
+        copy.wait()
+
+
+def exchange_weights(gate_weight, up_weight, down_weight):
+    size = lax.axis_size("sp")
+    depth, columns = gate_weight.shape
+    width = column_tiles(columns)[1] * 128
+    wide = jax.ShapeDtypeStruct((size * depth, width), gate_weight.dtype)
+    tall = jax.ShapeDtypeStruct((width, size * down_weight.shape[1]), down_weight.dtype)
+    pairs = pltpu.SemaphoreType.DMA((3, size - 1))
+    return pl.pallas_call(
+        functools.partial(weights_kernel, size, columns),
+        out_shape=(wide, wide, tall),
+        in_specs=[pl.BlockSpec(memory_space=pl.ANY)] * 3,
+        out_specs=[pl.BlockSpec(memory_space=pl.ANY)] * 3,
+        scratch_shapes=[pltpu.SemaphoreType.DMA((3, 2)), pairs, pairs, pairs, pairs],
+        compiler_params=pltpu.CompilerParams(collective_id=0, has_side_effects=True),
+        name="swap_weights",
+    )(gate_weight, up_weight, down_weight)
+
+
+def ffn_kernel(
+    size, own, gate_w, up_w, down_w, keep, mixed, out,
+    tokens, parts, from_core, from_x, from_z, total,
+    z_send, z_recv, x_send, x_recv, c_send, c_recv,
+    rc_send, rc_recv, rx_send, rx_recv, rz_send, rz_recv,
+):
+    here = lax.axis_index("sp")
+    t = lax.axis_index("tp")
+    core = t + 1 - 2 * lax.rem(t, 2)
+    across = t + 2 - 4 * lax.div(t, 2)
+    diagonal = core + 2 - 4 * lax.div(core, 2)
+    rows = own.shape[0]
+    to_core, to_x = {"tp": core}, {"tp": across}
+    signal_all(
+        [{"sp": lax.rem(here + shift, size)} for shift in range(1, size)] + [to_core, to_x]
+    )
+    z_copies = [None]
+    for shift in range(1, size):
+        copy = remote(
+            own,
+            tokens.at[here, t],
+            z_send.at[shift],
+            z_recv.at[shift],
+            {"sp": lax.rem(here + shift, size)},
+        )
+        copy.start()
+        z_copies.append(copy)
+    tokens[here, t] = own[...]
+    origins = [lax.rem(here - i + size, size) for i in range(size)]
+    pending = []
+    x_copies, c_first, c_second, r_first, r_second, rx, rz = {}, {}, {}, {}, {}, {}, {}
+
+    def start(table, i, *args):
+        copy = remote(*args)
+        copy.start()
+        table[i] = copy
+        pending.append(copy)
+
+    def step_a(i):
+        o = origins[i]
+        if i:
+            z_copies[i].wait_recv()
+        block = tokens.at[o, t] if i else own
+        start(x_copies, i, block, tokens.at[o, t], x_send.at[i], x_recv.at[i], to_x)
+        start(c_first, i, block, tokens.at[o, t], c_send.at[i, 0], c_recv.at[i, 0], to_core)
+
+    def step_b(i):
+        o = origins[i]
+        x_copies[i].wait_recv()
+        block = tokens.at[o, across]
+        start(c_second, i, block, block, c_send.at[i, 1], c_recv.at[i, 1], to_core)
+
+    def step_c(i):
+        o = origins[i]
+        c_first[i].wait_recv()
+        c_second[i].wait_recv()
+        x = tokens[o].reshape(4 * rows, own.shape[1])
+        gate = jnp.dot(x, gate_w[...], preferred_element_type=jnp.float32)
+        up = jnp.dot(x, up_w[...], preferred_element_type=jnp.float32)
+        hidden = (gate / (1.0 + jnp.exp(-gate)) * up * keep[...]).astype(jnp.bfloat16)
+        step = 512
+        for col in range(0, own.shape[1], step):
+            term = jnp.dot(
+                hidden, down_w[:, col : col + step], preferred_element_type=jnp.float32
+            )
+            parts[o, :, :, col : col + step] = term.astype(jnp.bfloat16).reshape(4, rows, step)
+        start(r_first, i, parts.at[o, diagonal], from_core.at[i, 1], rc_send.at[i, 1], rc_recv.at[i, 1], to_core)
+        start(r_second, i, parts.at[o, core], from_core.at[i, 0], rc_send.at[i, 0], rc_recv.at[i, 0], to_core)
+
+    def plus(one, two):
+        return one.astype(jnp.float32) + two.astype(jnp.float32)
+
+    def step_d(i):
+        o = origins[i]
+        r_first[i].wait_recv()
+        parts[o, across] = plus(parts[o, across], from_core[i, 1]).astype(jnp.bfloat16)
+        start(rx, i, parts.at[o, across], from_x.at[i], rx_send.at[i], rx_recv.at[i], to_x)
+        r_second[i].wait_recv()
+        parts[o, t] = plus(parts[o, t], from_core[i, 0]).astype(jnp.bfloat16)
+
+    def step_e(i):
+        o = origins[i]
+        rx[i].wait_recv()
+        if i == 0:
+            total[...] = mixed[...] + plus(parts[o, t], from_x[i])
+            return
+        parts[o, t] = plus(parts[o, t], from_x[i]).astype(jnp.bfloat16)
+        start(rz, i, parts.at[o, t], from_z.at[i], rz_send.at[i], rz_recv.at[i], {"sp": o})
+
+    steps = {"a": step_a, "b": step_b, "c": step_c, "d": step_d, "e": step_e}
+    last = size - 1
+    order = [("a", 0)]
+    for i in range(size + 2):
+        for name, lag in (("a", -1), ("b", 0), ("c", 0), ("d", 1), ("e", 2)):
+            if 0 <= i - lag <= last:
+                order.append((name, i - lag))
+    for name, i in order:
+        steps[name](i)
+    result = total[...]
+    for i in range(1, size):
+        rz[i].wait_recv()
+        result = result + from_z[i].astype(jnp.float32)
+    out[...] = result.astype(out.dtype)
+    for copy in z_copies[1:] + pending:
+        copy.wait_send()
+
+
+def spread_ffn(projected, residual, ffn_gain, swapped, hidden_columns):
+    size = lax.axis_size("sp")
+    own_rows = residual.shape[0] // lax.axis_size("tp")
+    tp_index = lax.axis_index("tp")
+    summed = lax.psum_scatter(projected, "tp", scatter_dimension=0, tiled=True)
+    residual_own = lax.dynamic_slice_in_dim(residual, tp_index * own_rows, own_rows, 0)
+    mixed_own = residual_own.astype(jnp.float32) + summed.astype(jnp.float32)
+    normed_own = norm_rows(mixed_own, ffn_gain).astype(jnp.bfloat16)
+    here = lax.axis_index("sp")
+    per = column_tiles(hidden_columns)[1]
+    before = jnp.where(here > 0, window_start(jnp.maximum(here - 1, 0), hidden_columns) + per, 0)
+    first = (before - window_start(here, hidden_columns)) * 128
+    keep = (jnp.arange(per * 128, dtype=jnp.int32) >= first).astype(jnp.float32)[None]
+    width = residual.shape[1]
+    block = (own_rows, width)
+    dma = pltpu.SemaphoreType.DMA
+    vmem = lambda *lead: pltpu.VMEM(lead + block, jnp.bfloat16)
+    pair = [dma((size,)), dma((size,))]
+    double = [dma((size, 2)), dma((size, 2))]
+    return pl.pallas_call(
+        functools.partial(ffn_kernel, size),
+        out_shape=jax.ShapeDtypeStruct(block, jnp.bfloat16),
+        in_specs=[pl.BlockSpec(memory_space=pltpu.VMEM)] * 6,
+        out_specs=pl.BlockSpec(memory_space=pltpu.VMEM),
+        scratch_shapes=[
+            vmem(size, 4), vmem(size, 4), vmem(size, 2), vmem(size), vmem(size),
+            pltpu.VMEM(block, jnp.float32),
+        ] + pair + pair + double + double + pair + pair,
+        compiler_params=pltpu.CompilerParams(collective_id=1, has_side_effects=True),
+        name="spread_ffn",
+    )(normed_own, *swapped, keep, mixed_own)
 
 
 def local(
@@ -44,6 +313,10 @@
     up_weight,
     down_weight,
 ):
+    sp_size = lax.axis_size("sp")
+    spread = spread_hidden(query_nope.shape[0] * sp_size, gate_weight.shape[1])
+    if spread:
+        swapped = exchange_weights(gate_weight, up_weight, down_weight)
     tok_rows = query_nope.shape[0]
     heads_here = query_nope.shape[1] // UNROTATED_SIZE
     own_rows = tok_rows // lax.axis_size("tp")
@@ -126,6 +399,8 @@
     projected = jnp.dot(attended, out_weight, preferred_element_type=jnp.float32).astype(
         jnp.bfloat16
     )
+    if spread:
+        return spread_ffn(projected, residual, ffn_gain, swapped, gate_weight.shape[1])
     summed = lax.psum(projected, "tp").astype(jnp.float32)
     mixed_all = residual.astype(jnp.float32) + summed
     normed_all = norm_rows(mixed_all, ffn_gain).astype(jnp.bfloat16)

time: 428 us -> 224 us (0.52)
  waiting for transfers between devices: 336 us -> 0.02 us
  Pallas kernels: 0 us -> 157 us
  matrix products: 31.9 us -> 7.43 us
    all_gather x3 -> x0, waiting for transfers between devices: 272 us -> none  [the longest x1 106 us: local(): lax.all_gather(down_weight, 'sp', axis=1, tiled=True)]
    pallas_call x0 -> x2, Pallas kernels: none -> 157 us  [the longest x1 96 us: spread_ffn(): pl.pallas_call(functools.partial(ffn_kernel, size), out_shape=jax.ShapeDt...]
    psum x1 -> x0, waiting for transfers between devices: 37.3 us -> none  [local(): summed = lax.psum(projected, 'tp').astype(jnp.float32)]
    reduce_scatter x1, waiting for transfers between devices: 24.8 us -> 0.01 us  [spread_ffn(): summed = lax.psum_scatter(projected, 'tp', scatter_dimension=0, tiled=True)]
    dot_general x2 -> x0, matrix products: 17.2 us -> none  [the longest x1 10.7 us: local(): jnp.dot(hidden, lax.all_gather(down_weight, 'sp', axis=1, tiled=True), pr...]
  transfers between devices with their start and end apart: 5 -> 1, of which waited for: 5 -> 0; matrix products, arithmetic and copies ran while one was open for 2% -> 0% of each run, Pallas kernels for 0% -> 27%
where the time goes in v1:
time: 224 us
  Pallas kernels  157 us (70%)
  blocking collectives  31.9 us (14%)
  between operations  13.6 us (6%)
  other arithmetic  8.21 us (4%)
  matrix products  7.43 us (3%)
  local copies, waits for them, and re-layouts  5.03 us (2%)
    pallas_call x1, Pallas kernels, spread_ffn(): pl.pallas_call(functools.partial(ffn_kernel, size), out_shape=jax.ShapeDt...  96 us
    pallas_call x1, Pallas kernels, exchange_weights(): pl.pallas_call(functools.partial(weights_kernel, size, columns), out_shap...  61.3 us
    all_gather x1, blocking collectives, local(): latent_piece = lax.all_gather(latent, 'sp', axis=0, tiled=True)  16.8 us
    all_gather x1, blocking collectives, local(): rope_piece = lax.all_gather(key_turned, 'sp', axis=0, tiled=True)  15.1 us
  transfers between devices with their start and end apart: 1, of which 0 were waited for; matrix products, arithmetic and copies ran while one was open for 0% of the time, Pallas kernels for 27%

profile of v1, /device:TPU:0, one launch (start us, length us, event | category | flops | bytes accessed | tf_op | source)
XLA Modules:
  0.0 223.8 jit_solution(635293781813267890)
XLA Ops:
  6.6 1.1 fusion.23
  7.8 0.7 convert.18
  8.9 15.1 %all-gather = bf16[4,320,32]{1,2,0:T(8,128)(2,1)S(1)} all-gather(bf16[1,320,32]{1,2,0:T(8,128)(2,1)S(1)} %bitcast.79), channel_id=1, replica_groups=mesh['grp'=2,'sp'=4,'tp'=4] {'sp'}, dimensions={0}, use_global_device_ids=true | all-gather | bytes 102400 | tf_op jit(solution)/shard_map/all_gather | solution.py:378
  24.2 1.0 copy.26
  25.2 1.1 copy.24
  26.3 1.0 fusion.25
  27.3 16.8 %all_gather.6 = bf16[1280,256]{1,0:T(8,128)(2,1)S(1)} all-gather(bf16[320,256]{1,0:T(8,128)(2,1)S(1)} %fusion.25), channel_id=1, replica_groups=mesh['grp'=2,'sp'=4,'tp'=4] {'sp'}, dimensions={0}, use_global_device_ids=true | all-gather | bytes 819200 | tf_op jit(solution)/shard_map/all_gather | solution.py:377
  44.2 1.0 constant_dynamic-slice_fusion
  45.2 8.1 %while.15 = (s32[]{:T(128)}, f32[4,320]{1,0:T(4,128)S(1)}, f32[4,320]{1,0:T(4,128)S(1)}, f32[320,4,64]{0,2,1:T(8,128)S(1)}, bf16[2,640,256]{2,1,0:T(8,128)(2,1)S...) while((s32[]{:T(128)}, f32[4,320]{1,0:T(4,128)S(1)}, ...), condition=%wide.region_4.5_spmd.clone, body=%wide.region_1.4_spmd.clone.sunk | while | flops 436231680 | bytes 19652756 | solution.py:392
  45.9 0.6 fusion.68
  46.5 0.8 fusion.69
  47.4 1.0 fusion.71
  48.3 0.8 fusion.73
  49.8 0.6 fusion.68
  50.5 0.8 fusion.69
  51.3 1.0 fusion.71
  52.3 0.8 fusion.73
  53.4 1.6 convolution_convert_fusion.2
  55.1 61.3 %swap_weights.1 = (bf16[2048,384]{1,0:T(8,128)(2,1)}, bf16[2048,384]{1,0:T(8,128)(2,1)}, bf16[384,2048]{1,0:T(8,128)(2,1)}) custom-call(bf16[512,1408]{1,0:T(8,128)(2,1)} %gate.1, bf16[512,1408]{1,0:T(8,128)(2,1)} %up.1, bf16[1408,512]{1,0:T(8,128)(2,1)} %down.1), custom_call_target="tpu_custom_call" | custom-call | tf_op jit(solution)/shard_map/swap_weights/pallas_call | solution.py:150
  116.4 0.6 compare_convert_fusion.keep
  117.0 1.3 multiply_reduce_fusion
  118.3 0.9 multiply_convert_fusion.own
  119.2 96.0 %spread_ffn.1 = bf16[80,2048]{1,0:T(8,128)(2,1)} custom-call(bf16[80,2048]{1,0:T(8,128)(2,1)} %multiply_convert_fusion.own, bf16[2048,384]{1,0:T(8,128)(2,1)} %get-tuple-element.63.gate_w, bf16[2048,384]{1,0:T(8,128)(2,1)} %get-tuple-element.64.up_w, bf16[384,2048]{1,0:T(8,128)(2,1)} %get-tuple-element.65.down_w, f32[1,384]{1,0:T(1,128)} %compare_convert_fusion.keep, ...), custom_call_target="tpu_custom_call" | custom-call | tf_op jit(solution)/shard_map/spread_ffn/pallas_call | solution.py:287
  215.2 1.7 copy.41
  (37 shorter events, 2.1 us)
Async XLA Ops:
  6.5 46.8 %copy-start = (bf16[256,2048]{1,0:T(8,128)(2,1)S(1)}, bf16[256,2048]{1,0:T(8,128)(2,1)}, u32[]{:S(2)}) copy-start(bf16[256,2048]{1,0:T(8,128)(2,1)} %param.23) | copy-start | bytes 3145732
  6.5 110.4 %reduce-scatter.2.cloned.1.call-start = ((), (), s32[]{:S(2)}) async-start(), calls=%async_computation.1 | async-start | bytes 1638400 | tf_op jit(solution)/shard_map/reduce_scatter | solution.py:272
  55.0 63.2 %copy-start.2 = (f32[2048]{0:T(1024)S(1)}, f32[2048]{0:T(1024)}, u32[]{:S(2)}) copy-start(f32[2048]{0:T(1024)} %param.24) | copy-start | bytes 24580
  118.2 1.0 copy-start.1
Sparse Core Ops, SparseCore 0:
  55.2 26.2 reduce-scatter.1

commit v2 on v1

--- a/solution.py
+++ b/solution.py
@@ -67,12 +67,18 @@
     )
 
 
-def weights_kernel(
-    size, hidden_columns, gate, up, down, gate_out, up_out, down_out,
-    own_sem, z_send, z_recv, y_send, y_recv,
+def front_kernel(
+    size, hidden_columns, query, turned, latent, key_w, value_w, out_w, residual, gain,
+    gate, up, down,
+    gate_out, up_out, down_out, mixed, normed,
+    gathered, projected, landed,
+    own_sem, z_send, z_recv, y_send, y_recv, l_send, l_recv, m_send, m_recv, r_send, r_recv,
 ):
     here = lax.axis_index("sp")
     part = lax.axis_index("grp")
+    t = lax.axis_index("tp")
+    side = lax.rem(t, 2)
+    core = t + 1 - 2 * side
     depth = gate.shape[0]
     width = gate_out.shape[1]
     outer = down.shape[1]
@@ -98,7 +104,22 @@
         return ref.at[pl.ds(pl.multiple_of(start_of(target) + half * rows, 64), rows), :]
 
     peers = [{"sp": lax.rem(here + shift, size)} for shift in range(1, size)]
+    peers += [{"tp": lax.rem(t + shift, 4)} for shift in range(1, 4)]
     signal_all(peers + [{"grp": 1 - part}])
+    tokens = latent.shape[0]
+    half_rows = tokens // 2
+    my_half = pl.ds(pl.multiple_of(side * half_rows, half_rows), half_rows)
+    spread_latent = []
+    for shift in range(1, size):
+        copy = remote(
+            latent.at[my_half, :],
+            gathered.at[here, my_half, :],
+            l_send.at[shift - 1],
+            l_recv.at[shift - 1],
+            {"sp": lax.rem(here + shift, size)},
+        )
+        copy.start()
+        spread_latent.append(copy)
     refs = ((gate, gate_out), (up, up_out), (down, down_out))
     across = []
     for kind, (ref, out) in enumerate(refs):
@@ -121,8 +142,78 @@
             )
             copy.start()
             locals_.append(copy)
+    gathered[here] = latent[...]
+    shared_latent = []
+    for shift in range(1, size):
+        spread_latent[shift - 1].wait_recv()
+        held = gathered.at[lax.rem(here - shift + size, size), my_half, :]
+        copy = remote(held, held, m_send.at[shift - 1], m_recv.at[shift - 1], {"tp": core})
+        copy.start()
+        shared_latent.append(copy)
+    for copy in shared_latent:
+        copy.wait_recv()
+
+    lanes = query.shape[1]
+    heads = lanes // UNROTATED_SIZE
+    rank = key_w.shape[0]
+    columns = pl.ds(pl.multiple_of(t * lanes, 128), lanes)
+    every = gathered[...].reshape(size * tokens, latent.shape[1])
+    every_latent = every[:, :rank]
+    keys = jnp.dot(every_latent, key_w[:, columns], preferred_element_type=jnp.float32)
+    values = jnp.dot(every_latent, value_w[:, columns], preferred_element_type=jnp.float32)
+    values = values.astype(jnp.bfloat16)
+    keys = jnp.concatenate([keys.astype(jnp.bfloat16), every[:, rank:]], axis=1)
+    scale = (UNROTATED_SIZE + ROPE) ** (-0.5)
+    lane = lax.broadcasted_iota(jnp.int32, (1, lanes), 1)
+    rope_lane = lax.broadcasted_iota(jnp.int32, (1, turned.shape[1]), 1)
+    attended = jnp.zeros((tokens, lanes), jnp.float32)
+    for head in range(heads):
+        mine = (lane >= head * UNROTATED_SIZE) & (lane < (head + 1) * UNROTATED_SIZE)
+        rope_mine = (rope_lane >= head * ROPE) & (rope_lane < (head + 1) * ROPE)
+        both = jnp.concatenate(
+            [
+                jnp.where(mine, query[...].astype(jnp.float32), 0.0),
+                jnp.where(rope_mine, turned[...].astype(jnp.float32), 0.0),
+            ],
+            axis=1,
+        ).astype(jnp.bfloat16)
+        scores = (
+            lax.dot_general(
+                both, keys, (((1,), (1,)), ((), ())), preferred_element_type=jnp.float32
+            )
+            * scale
+        )
+        raised = jnp.exp(scores - jnp.max(scores, axis=1, keepdims=True))
+        totals = jnp.sum(raised, axis=1, keepdims=True)
+        weighted = jnp.dot(
+            raised.astype(jnp.bfloat16), values, preferred_element_type=jnp.float32
+        )
+        attended = jnp.where(mine, weighted / totals, attended)
+    attended = attended.astype(jnp.bfloat16)
+    own_rows = mixed.shape[0]
+    step = 512
+    for col in range(0, out_w.shape[1], step):
+        term = jnp.dot(
+            attended, out_w[:, col : col + step], preferred_element_type=jnp.float32
+        )
+        projected[:, :, col : col + step] = term.astype(jnp.bfloat16).reshape(4, own_rows, step)
+    scattered = []
+    for shift in (2, 1, 3):
+        target = lax.rem(t + shift, 4)
+        copy = remote(
+            projected.at[target],
+            landed.at[shift - 1],
+            r_send.at[shift - 1],
+            r_recv.at[shift - 1],
+            {"tp": target},
+        )
+        copy.start()
+        scattered.append(copy)
+
     swaps = []
-    for kind, (ref, out) in enumerate(refs):
+
+    def forward(kind):
+        out = refs[kind][1]
         for shift in range(1, size):
             origin = lax.rem(here - shift + size, size)
             across[kind * (size - 1) + shift - 1].wait_recv()
@@ -132,7 +223,21 @@
             )
             copy.start()
             swaps.append(copy)
-    for copy in across:
+
+    forward(0)
+    forward(1)
+    for copy in scattered:
+        copy.wait_recv()
+    rows = pl.ds(pl.multiple_of(t * own_rows, own_rows), own_rows)
+    total = residual[rows, :].astype(jnp.float32) + projected[t].astype(jnp.float32)
+    for shift in range(3):
+        total = total + landed[shift].astype(jnp.float32)
+    mixed[...] = total
+    normed[...] = (
+        total * lax.rsqrt(jnp.mean(total * total, axis=1, keepdims=True) + 1e-06) * gain[...]
+    ).astype(jnp.bfloat16)
+    forward(2)
+    for copy in across + spread_latent + shared_latent + scattered:
         copy.wait_send()
     for copy in locals_:
         copy.wait()
@@ -140,22 +245,72 @@
         copy.wait()
 
 
-def exchange_weights(gate_weight, up_weight, down_weight):
+def front(query, turned, latent, key_w, value_w, out_w, residual, gain, gate, up, down):
     size = lax.axis_size("sp")
-    depth, columns = gate_weight.shape
+    depth, columns = gate.shape
     width = column_tiles(columns)[1] * 128
-    wide = jax.ShapeDtypeStruct((size * depth, width), gate_weight.dtype)
-    tall = jax.ShapeDtypeStruct((width, size * down_weight.shape[1]), down_weight.dtype)
-    pairs = pltpu.SemaphoreType.DMA((3, size - 1))
+    own = (residual.shape[0] // lax.axis_size("tp"), residual.shape[1])
+    wide = jax.ShapeDtypeStruct((size * depth, width), gate.dtype)
+    tall = jax.ShapeDtypeStruct((width, size * down.shape[1]), down.dtype)
+    dma = pltpu.SemaphoreType.DMA
+    pairs = dma((3, size - 1))
+    line = dma((size - 1,))
+    here = pl.BlockSpec(memory_space=pltpu.VMEM)
+    away = pl.BlockSpec(memory_space=pl.ANY)
     return pl.pallas_call(
-        functools.partial(weights_kernel, size, columns),
-        out_shape=(wide, wide, tall),
-        in_specs=[pl.BlockSpec(memory_space=pl.ANY)] * 3,
-        out_specs=[pl.BlockSpec(memory_space=pl.ANY)] * 3,
-        scratch_shapes=[pltpu.SemaphoreType.DMA((3, 2)), pairs, pairs, pairs, pairs],
+        functools.partial(front_kernel, size, columns),
+        out_shape=(
+            wide, wide, tall,
+            jax.ShapeDtypeStruct(own, jnp.float32), jax.ShapeDtypeStruct(own, jnp.bfloat16),
+        ),
+        in_specs=[here] * 8 + [away] * 3,
+        out_specs=[away] * 3 + [here] * 2,
+        scratch_shapes=[
+            pltpu.VMEM((size,) + latent.shape, jnp.bfloat16),
+            pltpu.VMEM((4,) + own, jnp.bfloat16),
+            pltpu.VMEM((3,) + own, jnp.bfloat16),
+            dma((3, 2)), pairs, pairs, pairs, pairs, line, line, line, line, dma((3,)), dma((3,)),
+        ],
         compiler_params=pltpu.CompilerParams(collective_id=0, has_side_effects=True),
-        name="swap_weights",
-    )(gate_weight, up_weight, down_weight)
+        name="front",
+    )(query, turned, latent, key_w, value_w, out_w, residual, gain, gate, up, down)
+
+
+def turn_lanes(vectors, positions):
+    lanes = vectors.shape[1]
+    freqs = ROPE // 4
+    lane = jnp.arange(lanes, dtype=jnp.int32)
+    inverse = jnp.power(10000.0, -(lane % freqs).astype(jnp.float32) / freqs)
+    first_axis = lane % ROPE < ROPE // 2
+    first_half = lane % (2 * freqs) < freqs
+    place = jnp.where(
+        first_axis[None], (positions // GRID_W)[:, None], (positions % GRID_W)[:, None]
+    )
+    angles = place.astype(jnp.float32) * inverse[None]
+    partner = jnp.where(first_half, lane + freqs, lane - freqs)
+    sign = jnp.where(first_half, -1.0, 1.0)
+    swap = jnp.where(lane[:, None] == partner[None], sign[None], 0.0).astype(vectors.dtype)
+    other = jnp.dot(vectors, swap, preferred_element_type=jnp.float32)
+    turned = vectors.astype(jnp.float32) * jnp.cos(angles) + other * jnp.sin(angles)
+    return turned.astype(jnp.bfloat16)
+
+
+def spread_layer(
+    query_nope, query_rope, token_latent, key_rope, latent_norm_gain, key_w, value_w,
+    residual, out_w, ffn_gain, gate_w, up_w, down_w,
+):
+    rows = query_nope.shape[0]
+    positions = lax.axis_index("sp") * rows + jnp.arange(rows, dtype=jnp.int32)
+    repeats = query_rope.shape[1] // ROPE
+    turned = turn_lanes(query_rope, positions)
+    key_turned = turn_lanes(jnp.tile(key_rope, (1, repeats)), positions)
+    latent = norm_rows(token_latent, latent_norm_gain).astype(jnp.bfloat16)
+    packed = jnp.concatenate([latent, key_turned], axis=1)
+    gate, up, down, mixed, normed = front(
+        query_nope, turned, packed, key_w, value_w, out_w, residual, ffn_gain[None],
+        gate_w, up_w, down_w,
+    )
+    return spread_ffn(normed, mixed, (gate, up, down), gate_w.shape[1])
 
 
 def ffn_kernel(
@@ -265,21 +420,14 @@
         copy.wait_send()
 
 
-def spread_ffn(projected, residual, ffn_gain, swapped, hidden_columns):
+def spread_ffn(normed_own, mixed_own, swapped, hidden_columns):
     size = lax.axis_size("sp")
-    own_rows = residual.shape[0] // lax.axis_size("tp")
-    tp_index = lax.axis_index("tp")
-    summed = lax.psum_scatter(projected, "tp", scatter_dimension=0, tiled=True)
-    residual_own = lax.dynamic_slice_in_dim(residual, tp_index * own_rows, own_rows, 0)
-    mixed_own = residual_own.astype(jnp.float32) + summed.astype(jnp.float32)
-    normed_own = norm_rows(mixed_own, ffn_gain).astype(jnp.bfloat16)
     here = lax.axis_index("sp")
     per = column_tiles(hidden_columns)[1]
     before = jnp.where(here > 0, window_start(jnp.maximum(here - 1, 0), hidden_columns) + per, 0)
     first = (before - window_start(here, hidden_columns)) * 128
     keep = (jnp.arange(per * 128, dtype=jnp.int32) >= first).astype(jnp.float32)[None]
-    width = residual.shape[1]
-    block = (own_rows, width)
+    block = normed_own.shape
     dma = pltpu.SemaphoreType.DMA
     vmem = lambda *lead: pltpu.VMEM(lead + block, jnp.bfloat16)
     pair = [dma((size,)), dma((size,))]
@@ -313,10 +461,22 @@
     up_weight,
     down_weight,
 ):
-    sp_size = lax.axis_size("sp")
-    spread = spread_hidden(query_nope.shape[0] * sp_size, gate_weight.shape[1])
-    if spread:
-        swapped = exchange_weights(gate_weight, up_weight, down_weight)
+    if spread_hidden(query_nope.shape[0] * lax.axis_size("sp"), gate_weight.shape[1]):
+        return spread_layer(
+            query_nope,
+            query_rope,
+            token_latent,
+            key_rope,
+            latent_norm_gain,
+            key_expand_weight,
+            value_expand_weight,
+            residual,
+            out_weight,
+            ffn_gain,
+            gate_weight,
+            up_weight,
+            down_weight,
+        )
     tok_rows = query_nope.shape[0]
     heads_here = query_nope.shape[1] // UNROTATED_SIZE
     own_rows = tok_rows // lax.axis_size("tp")
@@ -399,8 +559,6 @@
     projected = jnp.dot(attended, out_weight, preferred_element_type=jnp.float32).astype(
         jnp.bfloat16
     )
-    if spread:
-        return spread_ffn(projected, residual, ffn_gain, swapped, gate_weight.shape[1])
     summed = lax.psum(projected, "tp").astype(jnp.float32)
     mixed_all = residual.astype(jnp.float32) + summed
     normed_all = norm_rows(mixed_all, ffn_gain).astype(jnp.bfloat16)

time: 224 us -> 189 us (0.84)
  blocking collectives: 31.9 us -> 0 us
  Pallas kernels: 157 us -> 180 us
  between operations: 13.6 us -> 0.09 us
  matrix products: 7.43 us -> 2.09 us
  other arithmetic: 8.21 us -> 3.43 us
  local copies, waits for them, and re-layouts: 5.03 us -> 2.62 us
    all_gather x2 -> x0, blocking collectives: 31.9 us -> none  [the longest x1 16.8 us: local(): latent_piece = lax.all_gather(latent, 'sp', axis=0, tiled=True)]
    pallas_call x1, Pallas kernels: 61.3 us -> 82 us  [front(): pl.pallas_call(functools.partial(front_kernel, size, columns), out_shape=...]
    dot_general x11 -> x2, matrix products: 7.43 us -> 2.09 us  [turn_lanes(): other = jnp.dot(vectors, swap, preferred_element_type=jnp.float32)]
  transfers between devices with their start and end apart: 1 -> 0, of which waited for: 0 -> 0; matrix products, arithmetic and copies ran while one was open for 0% -> 0% of each run, Pallas kernels for 27% -> 0%
where the time goes in v2:
time: 189 us; the launch traced here: 188 us
  Pallas kernels  180 us (95%)
  other arithmetic  3.43 us (2%)
  local copies, waits for them, and re-layouts  2.62 us (1%)
  matrix products  2.09 us (1%)
    pallas_call x1, Pallas kernels, spread_ffn(): pl.pallas_call(functools.partial(ffn_kernel, size), out_shape=jax.ShapeDt...  98.2 us
    pallas_call x1, Pallas kernels, front(): pl.pallas_call(functools.partial(front_kernel, size, columns), out_shape=...  82 us

profile of v2, /device:TPU:0, one launch (start us, length us, event | category | flops | bytes accessed | tf_op | source)
XLA Modules:
  0.0 188.5 jit_solution(4504709269924091944)
XLA Ops:
  0.0 0.0 copy-start
  0.0 0.8 tile.4
  0.8 0.1 copy.15
  1.0 0.8 fusion.5
  1.7 1.1 fusion.6
  2.8 1.0 fusion.8
  3.8 0.7 pad_maximum_fusion.latent
  4.6 0.0 copy-done
  4.6 1.3 fusion.4.turned
  5.9 82.0 %front.1 = (bf16[2048,384]{1,0:T(8,128)(2,1)}, bf16[2048,384]{1,0:T(8,128)(2,1)}, bf16[384,2048]{1,0:T(8,128)(2,1)}, f32[80,2048]{1,0:T(8,128)}, bf16[80,2048]{1,0:T(8,128)(2,1)}) custom-call(bf16[320,256]{1,0:T(8,128)(2,1)} %query.1, bf16[320,128]{1,0:T(8,128)(2,1)} %fusion.4.turned, bf16[320,384]{1,0:T(8,128)(2,1)} %pad_maximum_fusion.latent, ...), custom_call_target="tpu_custom_call" | custom-call | tf_op jit(solution)/shard_map/front/pallas_call | solution.py:260
  88.0 0.6 compare_convert_fusion.keep
  88.5 98.2 %spread_ffn.1 = bf16[80,2048]{1,0:T(8,128)(2,1)} custom-call(bf16[80,2048]{1,0:T(8,128)(2,1)} %get-tuple-element.10.own, bf16[2048,384]{1,0:T(8,128)(2,1)} %get-tuple-element.11.gate_w, bf16[2048,384]{1,0:T(8,128)(2,1)} %get-tuple-element.12.up_w, bf16[384,2048]{1,0:T(8,128)(2,1)} %get-tuple-element.13.down_w, f32[1,384]{1,0:T(1,128)} %compare_convert_fusion.keep, ...), custom_call_target="tpu_custom_call" | custom-call | tf_op jit(solution)/shard_map/spread_ffn/pallas_call | solution.py:435
  186.7 1.7 copy.17
  (6 shorter events, 0.0 us)
Async XLA Ops:
  0.0 4.6 %copy-start = (bf16[320,128]{1,0:T(8,128)(2,1)S(1)}, bf16[320,128]{1,0:T(8,128)(2,1)}, u32[]{:S(2)}) copy-start(bf16[320,128]{1,0:T(8,128)(2,1)} %param.14) | copy-start | bytes 245764

commit v3 on v2

--- a/solution.py
+++ b/solution.py
@@ -405,8 +405,8 @@
     steps = {"a": step_a, "b": step_b, "c": step_c, "d": step_d, "e": step_e}
     last = size - 1
     order = [("a", 0)]
-    for i in range(size + 2):
-        for name, lag in (("a", -1), ("b", 0), ("c", 0), ("d", 1), ("e", 2)):
+    for i in range(size + 1):
+        for name, lag in (("a", -1), ("b", 0), ("c", 0), ("d", 0), ("e", 1)):
             if 0 <= i - lag <= last:
                 order.append((name, i - lag))
     for name, i in order:

time: 189 us -> 181 us (0.958)
  Pallas kernels: 180 us -> 173 us
    pallas_call x1, Pallas kernels: 98.2 us -> 90.6 us  [spread_ffn(): pl.pallas_call(functools.partial(ffn_kernel, size), out_shape=jax.ShapeDt...]
where the time goes in v3:
time: 181 us
  Pallas kernels  173 us (96%)
  other arithmetic  3.43 us (2%)
  local copies, waits for them, and re-layouts  2.62 us (1%)
  matrix products  2.09 us (1%)
    pallas_call x1, Pallas kernels, spread_ffn(): pl.pallas_call(functools.partial(ffn_kernel, size), out_shape=jax.ShapeDt...  90.6 us
    pallas_call x1, Pallas kernels, front(): pl.pallas_call(functools.partial(front_kernel, size, columns), out_shape=...  82 us

profile of v3, /device:TPU:0, one launch (start us, length us, event | category | flops | bytes accessed | tf_op | source)
XLA Modules:
  0.0 180.8 jit_solution(15174663605777799072)
XLA Ops:
  0.0 0.0 copy-start
  0.0 0.8 tile.4
  0.8 0.1 copy.15
  1.0 0.8 fusion.5
  1.7 1.1 fusion.6
  2.8 1.0 fusion.8
  3.8 0.7 pad_maximum_fusion.latent
  4.6 0.0 copy-done
  4.6 1.3 fusion.4.turned
  5.9 82.0 %front.1 = (bf16[2048,384]{1,0:T(8,128)(2,1)}, bf16[2048,384]{1,0:T(8,128)(2,1)}, bf16[384,2048]{1,0:T(8,128)(2,1)}, f32[80,2048]{1,0:T(8,128)}, bf16[80,2048]{1,0:T(8,128)(2,1)}) custom-call(bf16[320,256]{1,0:T(8,128)(2,1)} %query.1, bf16[320,128]{1,0:T(8,128)(2,1)} %fusion.4.turned, bf16[320,384]{1,0:T(8,128)(2,1)} %pad_maximum_fusion.latent, ...), custom_call_target="tpu_custom_call" | custom-call | tf_op jit(solution)/shard_map/front/pallas_call | solution.py:260
  88.0 0.6 compare_convert_fusion.keep
  88.5 90.6 %spread_ffn.1 = bf16[80,2048]{1,0:T(8,128)(2,1)} custom-call(bf16[80,2048]{1,0:T(8,128)(2,1)} %get-tuple-element.10.own, bf16[2048,384]{1,0:T(8,128)(2,1)} %get-tuple-element.11.gate_w, bf16[2048,384]{1,0:T(8,128)(2,1)} %get-tuple-element.12.up_w, bf16[384,2048]{1,0:T(8,128)(2,1)} %get-tuple-element.13.down_w, f32[1,384]{1,0:T(1,128)} %compare_convert_fusion.keep, ...), custom_call_target="tpu_custom_call" | custom-call | tf_op jit(solution)/shard_map/spread_ffn/pallas_call | solution.py:435
  179.1 1.7 copy.17
  (6 shorter events, 0.0 us)
Async XLA Ops:
  0.0 4.6 %copy-start = (bf16[320,128]{1,0:T(8,128)(2,1)S(1)}, bf16[320,128]{1,0:T(8,128)(2,1)}, u32[]{:S(2)}) copy-start(bf16[320,128]{1,0:T(8,128)(2,1)} %param.14) | copy-start | bytes 245764
